TPU v7x, 32 devices: a whole 2x2x4 slice. The times are simulated.
32 devices in a mesh: sp: 16 (over z, y, x), tp: 2 (over core).
Axes of the slice: x: 2, y: 2, z: 4, core: 2. Of those that a mesh axis runs over, the one named last changes fastest.
Arguments:
- value_in: bfloat16 [4096, 2048], P('sp', 'tp'), may hold values from -25 to 25, as said below
- gate_in: bfloat16 [4096, 2048], P('sp', 'tp'), may hold values from -6 to 6
- taps: float32 [31, 2048], P(None, 'tp'), may hold values from -1 to 1
- gain: float32 [2048], P('tp'), may hold values from 0.1 to 1.9
- shift: float32 [2048], P('tp'), may hold values from -3 to 3
- w_out: bfloat16 [2048, 2048], P('tp'), may hold values from -0.125 to 0.125
- grad_out: bfloat16 [4096, 2048], P('sp'), may hold values from -6 to 6
Outputs:
- d_value: bfloat16 [4096, 2048], P('sp', 'tp')
- d_gate: bfloat16 [4096, 2048], P('sp', 'tp')
- d_taps: float32 [31, 2048], P(None, 'tp')
- d_gain: float32 [2048], P('tp')
- d_shift: float32 [2048], P('tp')
Inputs may be any that keep to these rules, and one draw needn't show every extreme that they name: `value_in`: channel blocks of different magnitude.
All inputs are finite; a program needn't handle non-finite values.
Results may differ from a plain program's by a relative error of at most 0.007.
Values may be sent and summed in bfloat16 or wider, within the bound.
No kernel may reach another device: no remote copies, remote signals or barrier semaphores. Data moves between devices by JAX's collectives and lax.ppermute only.
A program may use at most 64 MiB of HBM per device.

v0:
```python
import math
import jax
import jax.numpy as jnp
from jax import lax
from jax.sharding import PartitionSpec as P

EPS = 1e-05


def with_halo(block, sides, width):
    for axis, dim in sides:
        count = lax.axis_size(axis)
        forward = [(i, i + 1) for i in range(count - 1)]
        backward = [(target, source) for source, target in forward]
        low = lax.ppermute(
            lax.slice_in_dim(block, block.shape[dim] - width, None, axis=dim), axis, forward
        )
        high = lax.ppermute(lax.slice_in_dim(block, 0, width, axis=dim), axis, backward)
        block = jnp.concatenate([low, block, high], axis=dim)
    return block


def gated_rows(value_rows, gate_rows):
    gate_sig = jax.nn.sigmoid(gate_rows.astype(jnp.float32))
    return ((value_rows.astype(jnp.float32) * gate_sig).astype(jnp.bfloat16), gate_sig)


def convolve(window, taps, count):
    wide = window.astype(jnp.float32)
    total = jnp.zeros((count, wide.shape[1]), jnp.float32)
    for offset in range(taps.shape[0]):
        total = total + taps[offset] * wide[offset : offset + count]
    return total


def norm_backward(conv_out, grad_rows, gain, shift, w_out, width):
    sums, squares = lax.psum((jnp.sum(conv_out, 1), jnp.sum(conv_out * conv_out, 1)), "tp")
    mean = sums / width
    var = squares / width - mean * mean
    inv = lax.rsqrt(var + EPS)
    normed = (conv_out - mean[:, None]) * inv[:, None]
    pre = normed * gain + shift
    grad_mix = lax.dot_general(
        grad_rows, w_out, (((1,), (1,)), ((), ())), preferred_element_type=jnp.float32
    )
    sig = jax.nn.sigmoid(pre)
    grad_pre = grad_mix * sig * (1.0 + pre * (1.0 - sig))
    grad_normed = grad_pre * gain
    first, second = lax.psum((jnp.sum(grad_normed, 1), jnp.sum(grad_normed * normed, 1)), "tp")
    grad_conv = inv[:, None] * (
        grad_normed - first[:, None] / width - normed * second[:, None] / width
    )
    return (grad_conv, grad_pre, normed)


def shards(value_in, gate_in, taps, gain, shift, w_out, grad_out):
    half = taps.shape[0] // 2
    kernel = taps.shape[0]
    rows = value_in.shape[0]
    width = value_in.shape[1] * lax.axis_size("tp")
    total = rows * lax.axis_size("sp")
    gated, gate_sig = gated_rows(value_in, gate_in)
    gated_wide = with_halo(gated, (("sp", 0),), half)
    conv_out = convolve(gated_wide, taps, rows)
    grad_conv, grad_pre, normed = norm_backward(conv_out, grad_out, gain, shift, w_out, width)
    grad_wide = with_halo(grad_conv, (("sp", 0),), half)
    own_grad = grad_wide[half : half + rows]
    gated_float = gated_wide.astype(jnp.float32)
    grad_gated = jnp.zeros((rows, own_grad.shape[1]), jnp.float32)
    for offset in range(kernel):
        grad_gated = (
            grad_gated + taps[offset] * grad_wide[2 * half - offset : 2 * half - offset + rows]
        )
    tap_terms = jnp.stack(
        [jnp.sum(own_grad * gated_float[offset : offset + rows], 0) for offset in range(kernel)]
    )
    scale = 1.0 / math.sqrt(total)
    stacked = (
        jnp.concatenate(
            [tap_terms, jnp.sum(grad_pre * normed, 0)[None], jnp.sum(grad_pre, 0)[None]], 0
        )
        * scale
    )
    summed = lax.psum(stacked, "sp")
    d_taps = summed[:kernel]
    d_gain = summed[kernel]
    d_shift = summed[kernel + 1]
    d_value = (grad_gated * gate_sig).astype(jnp.bfloat16)
    d_gate = (grad_gated * value_in.astype(jnp.float32) * gate_sig * (1.0 - gate_sig)).astype(
        jnp.bfloat16
    )
    return (d_value, d_gate, d_taps, d_gain, d_shift)


def solution(mesh):
    return jax.shard_map(
        shards,
        mesh=mesh,
        in_specs=(
            P("sp", "tp"),
            P("sp", "tp"),
            P(None, "tp"),
            P("tp"),
            P("tp"),
            P("tp", None),
            P("sp", None),
        ),
        out_specs=(P("sp", "tp"), P("sp", "tp"), P(None, "tp"), P("tp"), P("tp")),
        check_vma=False,
    )
```

profile of v0, /device:TPU:0, one launch (start us, length us, event | category | flops | bytes accessed | tf_op | source)
XLA Modules:
  0.0 175.2 jit_solution(298959568165321427)
XLA Ops:
  7.2 0.0 copy-start
  7.2 0.0 copy-start.4
  7.2 0.0 all-reduce.4.cloned.1.call-start
  7.2 1.6 fusion.1
  8.9 4.9 %collective-permute-start = (bf16[15,1024]{1,0:T(8,128)(2,1)S(1)}, bf16[15,1024]{1,0:T(8,128)(2,1)S(1)}, u32[]{:S(2)}, u32[]{:S(2)}) collective-permute-start(bf16[15,1024]{1,0:T(8,128)(2,1)S(1)} %get-tuple-element.52), channel_id=1, source_target_pairs={{0,2},{2,4},{4,6},{6,8},{8,10},{10,12},{12,14},{14,16},{16,18},{18... | collective-permute-start | bytes 92168 | tf_op jit(solution)/shard_map/ppermute | solution.py:15
  13.7 1.3 collective-permute-start.1
  15.0 0.0 copy-done.4
  15.0 0.1 fusion.97
  15.1 0.0 copy-start.5
  15.1 0.0 copy-start.6
  15.1 0.0 copy-start.7
  15.1 0.0 copy-start.8
  15.1 0.0 copy-start.9
  15.2 0.0 copy-start.10
  15.2 0.0 copy-start.11
  15.2 0.0 copy-start.12
  15.2 0.0 copy-start.13
  15.2 0.0 copy-start.14
  15.3 0.0 copy-start.15
  15.3 0.0 copy-start.16
  15.3 0.0 copy-start.17
  15.3 0.0 copy-start.18
  15.3 0.0 copy-start.19
  15.3 0.0 collective-permute-done
  15.4 4.2 %collective-permute-done.1 = bf16[15,1024]{1,0:T(8,128)(2,1)S(1)} collective-permute-done((bf16[15,1024]{1,0:T(8,128)(2,1)S(1)}, bf16[15,1024]{1,0:T(8,128)(2,1)S(1)}, u32[]{:S(2)}, u32[]{:S(2)}) %collective-permute-start.1) | collective-permute-done | bytes 30752 | tf_op jit(solution)/shard_map/ppermute | solution.py:18
  19.5 0.2 maximum_convert_fusion
  19.7 0.0 copy-start.24
  19.7 0.0 copy-start.25
  19.7 5.7 %multiply_reduce_fusion.33 = (f32[256]{0:T(256)S(1)}, f32[256]{0:T(256)S(1)}, f32[256,1024]{1,0:T(8,128)S(1)}) fusion(f32[286,1024]{1,0:T(8,128)S(1)} %maximum_convert_fusion, f32[1024]{0:T(1024)S(1)} %bitcast.126, f32[1024]{0:T(1024)S(1)} %bitcast.128, f32[1024]{0:T(1024)S(1)} %bitcast.70, f32[1024]{0:T(1024)S(1)} %bitcast.72, f32[1024]{0:T(1024)S(1)} %bitcast.74, ...), kind=kLoop, calls=%fused_computation.186 | loop fusion | flops 16776704 | bytes 33683456 | tf_op jit(solution)/shard_map/reduce_sum | solution.py:37
  25.6 2.5 %all-reduce.1 = (f32[256]{0:T(256)S(1)}, f32[256]{0:T(256)S(1)}) all-reduce(f32[256]{0:T(256)S(1)} %get-tuple-element.41, f32[256]{0:T(256)S(1)} %get-tuple-element.40), channel_id=1, replica_groups=mesh['sp'=16,'tp'=2] {'tp'}, use_global_device_ids=true, to_apply=%region_3.0 | all-reduce | flops 512 | bytes 4096 | tf_op jit(solution)/shard_map/psum | solution.py:37
  28.1 0.0 copy-done
  28.1 5.5 %multiply_reduce_fusion = (f32[1024]{0:T(1024)}, f32[256]{0:T(256)S(1)}, f32[256]{0:T(256)S(1)}, f32[1024]{0:T(1024)}, f32[256,1024]{1,0:T(8,128)}) fusion(f32[256,1024]{1,0:T(8,128)S(1)} %get-tuple-element.49, f32[256]{0:T(256)S(1)} %get-tuple-element.88, f32[256]{0:T(256)S(1)} %get-tuple-element.87, f32[1024]{0:T(1024)S(1)} %copy-done.24, ...), kind=kOutput, calls=%fused_computation.150 | convolution fusion | flops 1078720000 | bytes 7360512 | tf_op jit(solution)/shard_map/dot_general | solution.py:43
  33.7 2.4 %all-reduce = (f32[256]{0:T(256)S(1)}, f32[256]{0:T(256)S(1)}) all-reduce(f32[256]{0:T(256)S(1)} %get-tuple-element.37, f32[256]{0:T(256)S(1)} %get-tuple-element.38), channel_id=1, replica_groups=mesh['sp'=16,'tp'=2] {'tp'}, use_global_device_ids=true, to_apply=%region_7.0 | all-reduce | flops 512 | bytes 4096 | tf_op jit(solution)/shard_map/psum | solution.py:49
  36.1 4.8 %multiply_reduce_fusion.1 = (f32[1024]{0:T(1024)}, f32[1024]{0:T(1024)}, f32[1024]{0:T(1024)}, f32[1024]{0:T(1024)}, f32[1024]{0:T(1024)}, /*index=5*/f32[1024]{...) fusion(f32[286,1024]{1,0:T(8,128)S(1)} %maximum_convert_fusion,, ...), kind=kLoop, calls=%fused_computation.151 | loop fusion | flops 11515904 | bytes 22102016 | tf_op jit(solution)/shard_map/reduce_sum | solution.py:75
  41.0 2.4 %multiply_reduce_fusion.2 = (f32[1024]{0:T(1024)}, f32[1024]{0:T(1024)}, f32[1024]{0:T(1024)}, f32[1024]{0:T(1024)}, f32[1024]{0:T(1024)}, /*index=5*/f32[1024]{...) fusion(f32[256,1024]{1,0:T(8,128)S(1)} %get-tuple-element.46, ...), kind=kLoop, calls=%fused_computation.152 | loop fusion | flops 6802432 | bytes 14733312 | tf_op jit(solution)/shard_map/reduce_sum | solution.py:75
  43.3 0.6 fusion.94
  44.0 1.3 collective-permute-start.2
  45.3 4.9 %collective-permute-start.3 = (f32[15,1024]{1,0:T(8,128)S(1)}, f32[15,1024]{1,0:T(8,128)S(1)}, u32[]{:S(2)}, u32[]{:S(2)}) collective-permute-start(f32[15,1024]{1,0:T(8,128)S(1)} %get-tuple-element.51), channel_id=1, source_target_pairs={{0,2},{2,4},{4,6},{6,8},{8,10},{10,12},{12,14},{14,16},{16,18},{18... | collective-permute-start | bytes 184328 | tf_op jit(solution)/shard_map/ppermute | solution.py:15
  50.2 3.8 %concatenate.44 = f32[33,1024]{1,0:T(8,128)S(1)} concatenate(f32[1,1024]{1,0:T(1,128)} %bitcast.160, f32[1,1024]{1,0:T(1,128)} %bitcast.159, f32[1,1024]{1,0:T(1,128)} %bitcast.158, f32[1,1024]{1,0:T(1,128)} %bitcast.157, f32[1,1024]{1,0:T(1,128)} %bitcast.156, f32[1,1024]{1,0:T(1,128)} %bitcast.155, f32[1,1024]{1,0:T(1,128)} %bitcast.154, f32[1,1024]{1,0:T(1,128)} %bitcast.153, ...), dimensions={0} | concatenate | bytes 270336 | tf_op jit(solution)/shard_map/concatenate | solution.py:79
  54.0 0.7 broadcast_multiply_fusion
  54.7 0.0 all-reduce.4.cloned.1.call-update
  54.7 0.0 collective-permute-done.2
  54.7 0.0 collective-permute-done.3
  54.8 6.9 %fusion.4 = (bf16[256,1024]{1,0:T(8,128)(2,1)}, f32[256,1024]{1,0:T(8,128)}) fusion(bf16[256,1024]{1,0:T(8,128)(2,1)S(1)} %copy-done.3, bf16[256,1024]{1,0:T(8,128)(2,1)S(1)} %copy-done.1, f32[256,1024]{1,0:T(8,128)S(1)} %get-tuple-element.46, f32[15,1024]{1,0:T(8,128)S(1)} %collective-permute-done.3, f32[1024]{0:T(1024)} %bitcast.127, f32[1024]{0:T(1024)} %bitcast.129, ...), kind=kLoop, calls=%fused_computation.35 | loop fusion | flops 26476544 | bytes 3919872 | tf_op jit(solution)/shard_map/convert_element_type | solution.py:89
  61.7 2.3 %multiply_convert_fusion = bf16[256,1024]{1,0:T(8,128)(2,1)} fusion(f32[256,1024]{1,0:T(8,128)} %get-tuple-element.48, bf16[256,1024]{1,0:T(8,128)(2,1)S(1)} %copy-done.1), kind=kLoop, calls=%fused_computation.182 | loop fusion | flops 1572864 | bytes 2097152 | tf_op jit(solution)/shard_map/convert_element_type | solution.py:88
  64.0 101.4 %all-reduce.4.cloned.1.call-done = f32[33,1024]{1,0:T(8,128)} async-done(((f32[33,1024]{1,0:T(8,128)}), f32[33,1024]{1,0:T(8,128)}) %all-reduce.4.cloned.1.call-update) | async-done | bytes 135184 | tf_op jit(solution)/shard_map/psum | solution.py:84
  165.4 1.4 fusion.96
  166.8 1.6 slice.579
  (35 shorter events, 0.1 us)
Async XLA Ops:
  7.2 20.9 %copy-start = (bf16[256,2048]{1,0:T(8,128)(2,1)S(1)}, bf16[256,2048]{1,0:T(8,128)(2,1)}, u32[]{:S(2)}) copy-start(bf16[256,2048]{1,0:T(8,128)(2,1)} %param.13) | copy-start | bytes 3145732
  7.2 7.9 %copy-start.4 = (f32[31,1024]{1,0:T(8,128)S(1)}, f32[31,1024]{1,0:T(8,128)}, u32[]{:S(2)}) copy-start(f32[31,1024]{1,0:T(8,128)} %param.9) | copy-start | bytes 380932
  7.2 158.2 %all-reduce.4.cloned.1.call-start = ((), (), s32[]{:S(2)}) async-start(), calls=%async_computation | async-start | bytes 327680 | tf_op jit(solution)/shard_map/psum | solution.py:84
  8.9 6.5 %collective-permute-start = (bf16[15,1024]{1,0:T(8,128)(2,1)S(1)}, bf16[15,1024]{1,0:T(8,128)(2,1)S(1)}, u32[]{:S(2)}, u32[]{:S(2)}) collective-permute-start(bf16[15,1024]{1,0:T(8,128)(2,1)S(1)} %get-tuple-element.52), channel_id=1, source_target_pairs={{0,2},{2,4},{4,6},{6,8},{8,10},{10,12},{12,14},{14,16},{16,18},{18... | collective-permute-start | bytes 92168 | tf_op jit(solution)/shard_map/ppermute | solution.py:15
  13.7 5.8 %collective-permute-start.1 = (bf16[15,1024]{1,0:T(8,128)(2,1)S(1)}, bf16[15,1024]{1,0:T(8,128)(2,1)S(1)}, u32[]{:S(2)}, u32[]{:S(2)}) collective-permute-start(bf16[15,1024]{1,0:T(8,128)(2,1)S(1)} %get-tuple-element.53), channel_id=1, source_target_pairs={{2,0},{4,2},{6,4},{8,6},{10,8},{12,10},{14,12},{16,14},{18,16},{20... | collective-permute-start | bytes 92168 | tf_op jit(solution)/shard_map/ppermute | solution.py:18
  15.1 10.3 %copy-start.5 = (f32[1,1024]{1,0:T(1,128)}, f32[1,1024]{1,0:T(1,128)S(1)}, u32[]{:S(2)}) copy-start(f32[1,1024]{1,0:T(1,128)S(1)} %get-tuple-element.68) | copy-start | bytes 12292
  15.1 10.3 %copy-start.6 = (f32[1,1024]{1,0:T(1,128)}, f32[1,1024]{1,0:T(1,128)S(1)}, u32[]{:S(2)}) copy-start(f32[1,1024]{1,0:T(1,128)S(1)} %get-tuple-element.69) | copy-start | bytes 12292
  15.1 10.3 %copy-start.7 = (f32[1,1024]{1,0:T(1,128)}, f32[1,1024]{1,0:T(1,128)S(1)}, u32[]{:S(2)}) copy-start(f32[1,1024]{1,0:T(1,128)S(1)} %get-tuple-element.70) | copy-start | bytes 12292
  15.1 10.3 %copy-start.8 = (f32[1,1024]{1,0:T(1,128)}, f32[1,1024]{1,0:T(1,128)S(1)}, u32[]{:S(2)}) copy-start(f32[1,1024]{1,0:T(1,128)S(1)} %get-tuple-element.71) | copy-start | bytes 12292
  15.1 10.3 %copy-start.9 = (f32[1,1024]{1,0:T(1,128)}, f32[1,1024]{1,0:T(1,128)S(1)}, u32[]{:S(2)}) copy-start(f32[1,1024]{1,0:T(1,128)S(1)} %get-tuple-element.72) | copy-start | bytes 12292
  15.2 10.3 %copy-start.10 = (f32[1,1024]{1,0:T(1,128)}, f32[1,1024]{1,0:T(1,128)S(1)}, u32[]{:S(2)}) copy-start(f32[1,1024]{1,0:T(1,128)S(1)} %get-tuple-element.73) | copy-start | bytes 12292
  15.2 10.3 %copy-start.11 = (f32[1,1024]{1,0:T(1,128)}, f32[1,1024]{1,0:T(1,128)S(1)}, u32[]{:S(2)}) copy-start(f32[1,1024]{1,0:T(1,128)S(1)} %get-tuple-element.74) | copy-start | bytes 12292
  15.2 10.3 %copy-start.12 = (f32[1,1024]{1,0:T(1,128)}, f32[1,1024]{1,0:T(1,128)S(1)}, u32[]{:S(2)}) copy-start(f32[1,1024]{1,0:T(1,128)S(1)} %get-tuple-element.75) | copy-start | bytes 12292
  15.2 10.3 %copy-start.13 = (f32[1,1024]{1,0:T(1,128)}, f32[1,1024]{1,0:T(1,128)S(1)}, u32[]{:S(2)}) copy-start(f32[1,1024]{1,0:T(1,128)S(1)} %get-tuple-element.76) | copy-start | bytes 12292
  15.2 10.3 %copy-start.14 = (f32[1,1024]{1,0:T(1,128)}, f32[1,1024]{1,0:T(1,128)S(1)}, u32[]{:S(2)}) copy-start(f32[1,1024]{1,0:T(1,128)S(1)} %get-tuple-element.77) | copy-start | bytes 12292
  15.3 10.3 %copy-start.15 = (f32[1,1024]{1,0:T(1,128)}, f32[1,1024]{1,0:T(1,128)S(1)}, u32[]{:S(2)}) copy-start(f32[1,1024]{1,0:T(1,128)S(1)} %get-tuple-element.78) | copy-start | bytes 12292
  15.3 10.3 %copy-start.16 = (f32[1,1024]{1,0:T(1,128)}, f32[1,1024]{1,0:T(1,128)S(1)}, u32[]{:S(2)}) copy-start(f32[1,1024]{1,0:T(1,128)S(1)} %get-tuple-element.79) | copy-start | bytes 12292
  15.3 10.3 %copy-start.17 = (f32[1,1024]{1,0:T(1,128)}, f32[1,1024]{1,0:T(1,128)S(1)}, u32[]{:S(2)}) copy-start(f32[1,1024]{1,0:T(1,128)S(1)} %get-tuple-element.80) | copy-start | bytes 12292
  15.3 10.3 %copy-start.18 = (f32[1,1024]{1,0:T(1,128)}, f32[1,1024]{1,0:T(1,128)S(1)}, u32[]{:S(2)}) copy-start(f32[1,1024]{1,0:T(1,128)S(1)} %get-tuple-element.81) | copy-start | bytes 12292
  15.3 10.3 %copy-start.19 = (f32[1,1024]{1,0:T(1,128)}, f32[1,1024]{1,0:T(1,128)S(1)}, u32[]{:S(2)}) copy-start(f32[1,1024]{1,0:T(1,128)S(1)} %get-tuple-element.82) | copy-start | bytes 12292
  15.3 10.3 %copy-start.20 = (f32[1,1024]{1,0:T(1,128)}, f32[1,1024]{1,0:T(1,128)S(1)}, u32[]{:S(2)}) copy-start(f32[1,1024]{1,0:T(1,128)S(1)} %get-tuple-element.83) | copy-start | bytes 12292
  15.3 10.3 %copy-start.21 = (f32[1,1024]{1,0:T(1,128)}, f32[1,1024]{1,0:T(1,128)S(1)}, u32[]{:S(2)}) copy-start(f32[1,1024]{1,0:T(1,128)S(1)} %get-tuple-element.84) | copy-start | bytes 12292
  15.3 10.3 %copy-start.22 = (f32[1,1024]{1,0:T(1,128)}, f32[1,1024]{1,0:T(1,128)S(1)}, u32[]{:S(2)}) copy-start(f32[1,1024]{1,0:T(1,128)S(1)} %get-tuple-element.85) | copy-start | bytes 12292
  15.3 10.3 %copy-start.23 = (f32[1,1024]{1,0:T(1,128)}, f32[1,1024]{1,0:T(1,128)S(1)}, u32[]{:S(2)}) copy-start(f32[1,1024]{1,0:T(1,128)S(1)} %get-tuple-element.86) | copy-start | bytes 12292
  19.7 8.4 %copy-start.24 = (f32[1024]{0:T(1024)S(1)}, f32[1024]{0:T(1024)}, u32[]{:S(2)}) copy-start(f32[1024]{0:T(1024)} %param.10) | copy-start | bytes 12292
  19.7 8.4 %copy-start.25 = (f32[1024]{0:T(1024)S(1)}, f32[1024]{0:T(1024)}, u32[]{:S(2)}) copy-start(f32[1024]{0:T(1024)} %param.11) | copy-start | bytes 12292
  25.6 8.0 %copy-start.2 = (f32[256,1024]{1,0:T(8,128)}, f32[256,1024]{1,0:T(8,128)S(1)}, u32[]{:S(2)}) copy-start(f32[256,1024]{1,0:T(8,128)S(1)} %get-tuple-element.49) | copy-start | bytes 3145732
  43.3 11.4 %copy-start.1 = (bf16[256,1024]{1,0:T(8,128)(2,1)S(1)}, bf16[256,1024]{1,0:T(8,128)(2,1)}, u32[]{:S(2)}) copy-start(bf16[256,1024]{1,0:T(8,128)(2,1)} %param.8) | copy-start | bytes 1572868
  43.3 11.4 %copy-start.3 = (bf16[256,1024]{1,0:T(8,128)(2,1)S(1)}, bf16[256,1024]{1,0:T(8,128)(2,1)}, u32[]{:S(2)}) copy-start(bf16[256,1024]{1,0:T(8,128)(2,1)} %param.7) | copy-start | bytes 1572868
  44.0 10.7 %collective-permute-start.2 = (f32[15,1024]{1,0:T(8,128)}, f32[15,1024]{1,0:T(8,128)S(1)}, u32[]{:S(2)}, u32[]{:S(2)}) collective-permute-start(f32[15,1024]{1,0:T(8,128)} %get-tuple-element.50), channel_id=1, source_target_pairs={{2,0},{4,2},{6,4},{8,6},{10,8},{12,10},{14,12},{16,14},{18,16},{20... | collective-permute-start | bytes 184328 | tf_op jit(solution)/shard_map/ppermute | solution.py:18
  45.3 9.5 %collective-permute-start.3 = (f32[15,1024]{1,0:T(8,128)S(1)}, f32[15,1024]{1,0:T(8,128)S(1)}, u32[]{:S(2)}, u32[]{:S(2)}) collective-permute-start(f32[15,1024]{1,0:T(8,128)S(1)} %get-tuple-element.51), channel_id=1, source_target_pairs={{0,2},{2,4},{4,6},{6,8},{8,10},{10,12},{12,14},{14,16},{16,18},{18... | collective-permute-start | bytes 184328 | tf_op jit(solution)/shard_map/ppermute | solution.py:15
Sparse Core Ops, SparseCore 0:
  54.8 110.4 all-reduce.3
where the time goes:
time: 176 us; the launch traced here: 175 us
  waiting for transfers between devices  106 us (60%)
  other arithmetic  24.5 us (14%)
  between operations  14.5 us (8%)
  starting transfers between devices  12.4 us (7%)
  local copies, waits for them, and re-layouts  7.63 us (4%)
  matrix products  5.53 us (3%)
  blocking collectives  4.91 us (3%)
    psum x1, waiting for transfers between devices, shards(): summed = lax.psum(stacked, 'sp')  101 us
    ppermute x2, starting transfers between devices, with_halo(): lax.ppermute(lax.slice_in_dim(block, block.shape[dim] - width, None, axis...  9.8 us
    reduce_sum x2, other arithmetic, shards(): jnp.sum(own_grad * gated_float[offset:offset + rows], 0)  7.23 us
    convert_element_type x1, other arithmetic, shards(): (grad_gated * value_in.astype(jnp.float32) * gate_sig * (1.0 - gate_sig))...  6.89 us
    reduce_sum x1, other arithmetic, norm_backward(): jnp.sum(conv_out * conv_out, 1)  5.69 us
    dot_general x1, matrix products, norm_backward(): lax.dot_general(grad_rows, w_out, (((1,), (1,)), ((), ())), preferred_ele...  5.53 us
    ppermute x2, waiting for transfers between devices, with_halo(): lax.ppermute(lax.slice_in_dim(block, 0, width, axis=dim), axis, backward)  4.19 us
    concatenate x1, local copies, waits for them, and re-layouts, shards(): jnp.concatenate([tap_terms, jnp.sum(grad_pre * normed, 0)[None], jnp.sum(...  3.82 us
  transfers between devices with their start and end apart: 5, of which 2 were waited for; matrix products, arithmetic and copies ran while one was open for 8% of the time, Pallas kernels for 0%

commit v1 on v0

--- a/solution.py
+++ b/solution.py
@@ -81,7 +81,9 @@
         )
         * scale
     )
-    summed = lax.psum(stacked, "sp")
+    summed = stacked
+    for hop in (1, 2, 4, 8):
+        summed = summed + lax.ppermute(summed, "sp", [(dev, dev ^ hop) for dev in range(16)])
     d_taps = summed[:kernel]
     d_gain = summed[kernel]
     d_shift = summed[kernel + 1]

time: 176 us -> 78.8 us (0.45)
  waiting for transfers between devices: 106 us -> 12.6 us
  between operations: 14.5 us -> 0.86 us
  starting transfers between devices: 12.4 us -> 24.5 us
  local copies, waits for them, and re-layouts: 7.63 us -> 5.38 us
    psum x1 -> x0, waiting for transfers between devices: 101 us -> none  [shards(): summed = lax.psum(stacked, 'sp')]
    ppermute x0 -> x4, starting transfers between devices: none -> 12.5 us  [shards(): lax.ppermute(summed, 'sp', [(dev, dev ^ hop) for dev in range(16)])]
    ppermute x0 -> x4, waiting for transfers between devices: none -> 7.99 us  [shards(): lax.ppermute(summed, 'sp', [(dev, dev ^ hop) for dev in range(16)])]
  transfers between devices with their start and end apart: 5 -> 8, of which waited for: 2 -> 5; matrix products, arithmetic and copies ran while one was open for 8% -> 11% of each run, Pallas kernels for 0% -> 0%
where the time goes in v1:
time: 78.8 us; the launch traced here: 78.3 us
  other arithmetic  24.6 us (31%)
  starting transfers between devices  24.5 us (31%)
  waiting for transfers between devices  12.6 us (16%)
  matrix products  5.53 us (7%)
  local copies, waits for them, and re-layouts  5.38 us (7%)
  blocking collectives  4.91 us (6%)
  between operations  0.86 us (1%)
    ppermute x4, starting transfers between devices, shards(): lax.ppermute(summed, 'sp', [(dev, dev ^ hop) for dev in range(16)])  12.5 us
    ppermute x2, starting transfers between devices, with_halo(): lax.ppermute(lax.slice_in_dim(block, block.shape[dim] - width, None, axis...  9.42 us
    ppermute x4, waiting for transfers between devices, shards(): lax.ppermute(summed, 'sp', [(dev, dev ^ hop) for dev in range(16)])  7.99 us
    reduce_sum x2, other arithmetic, shards(): jnp.sum(own_grad * gated_float[offset:offset + rows], 0)  7.23 us
    convert_element_type x1, other arithmetic, shards(): (grad_gated * value_in.astype(jnp.float32) * gate_sig * (1.0 - gate_sig))...  6.57 us
    reduce_sum x1, other arithmetic, norm_backward(): jnp.sum(conv_out * conv_out, 1)  5.69 us
    dot_general x1, matrix products, norm_backward(): lax.dot_general(grad_rows, w_out, (((1,), (1,)), ((), ())), preferred_ele...  5.53 us
    ppermute x2, waiting for transfers between devices, with_halo(): lax.ppermute(lax.slice_in_dim(block, 0, width, axis=dim), axis, backward)  4.23 us
  transfers between devices with their start and end apart: 8, of which 5 were waited for; matrix products, arithmetic and copies ran while one was open for 11% of the time, Pallas kernels for 0%

profile of v1, /device:TPU:0, one launch (start us, length us, event | category | flops | bytes accessed | tf_op | source)
XLA Modules:
  0.0 78.3 jit_solution(14285861433512021233)
XLA Ops:
  0.6 0.0 copy-start
  0.6 0.0 copy-start.4
  0.7 1.6 %fusion.1 = bf16[256,1024]{1,0:T(8,128)(2,1)S(1)} fusion(bf16[256,1024]{1,0:T(8,128)(2,1)} %param.7, bf16[256,1024]{1,0:T(8,128)(2,1)} %param.8), kind=kLoop, calls=%fused_computation.32 | loop fusion | flops 1835008 | bytes 1572864 | tf_op jit(solution)/shard_map/convert_element_type | solution.py:25
  2.3 4.9 %collective-permute-start = (bf16[15,1024]{1,0:T(8,128)(2,1)S(1)}, bf16[15,1024]{1,0:T(8,128)(2,1)S(1)}, u32[]{:S(2)}, u32[]{:S(2)}) collective-permute-start(bf16[15,1024]{1,0:T(8,128)(2,1)S(1)} %get-tuple-element.52), channel_id=1, source_target_pairs={{0,2},{2,4},{4,6},{6,8},{8,10},{10,12},{12,14},{14,16},{16,18},{18... | collective-permute-start | bytes 92168 | tf_op jit(solution)/shard_map/ppermute | solution.py:15
  7.2 1.3 %collective-permute-start.1 = (bf16[15,1024]{1,0:T(8,128)(2,1)S(1)}, bf16[15,1024]{1,0:T(8,128)(2,1)S(1)}, u32[]{:S(2)}, u32[]{:S(2)}) collective-permute-start(bf16[15,1024]{1,0:T(8,128)(2,1)S(1)} %get-tuple-element.53), channel_id=1, source_target_pairs={{2,0},{4,2},{6,4},{8,6},{10,8},{12,10},{14,12},{16,14},{18,16},{20... | collective-permute-start | bytes 92168 | tf_op jit(solution)/shard_map/ppermute | solution.py:18
  8.5 0.0 copy-done.4
  8.5 0.1 fusion.98
  8.6 0.0 copy-start.5
  8.6 0.0 copy-start.6
  8.6 0.0 copy-start.7
  8.6 0.1 collective-permute-done
  8.8 4.2 %collective-permute-done.1 = bf16[15,1024]{1,0:T(8,128)(2,1)S(1)} collective-permute-done((bf16[15,1024]{1,0:T(8,128)(2,1)S(1)}, bf16[15,1024]{1,0:T(8,128)(2,1)S(1)}, u32[]{:S(2)}, u32[]{:S(2)}) %collective-permute-start.1) | collective-permute-done | bytes 30752 | tf_op jit(solution)/shard_map/ppermute | solution.py:18
  13.0 0.2 maximum_convert_fusion
  13.1 0.0 copy-start.8
  13.2 0.0 copy-start.9
  13.2 5.7 %multiply_reduce_fusion.33 = (f32[256]{0:T(256)S(1)}, f32[256]{0:T(256)S(1)}, f32[256,1024]{1,0:T(8,128)S(1)}) fusion(f32[286,1024]{1,0:T(8,128)S(1)} %maximum_convert_fusion, f32[1024]{0:T(1024)S(1)} %bitcast.126, f32[1024]{0:T(1024)S(1)} %bitcast.128, f32[1024]{0:T(1024)S(1)} %bitcast.70, f32[1024]{0:T(1024)S(1)} %bitcast.72, f32[1024]{0:T(1024)S(1)} %bitcast.74, ...), kind=kLoop, calls=%fused_computation.186 | loop fusion | flops 16776704 | bytes 33683456 | tf_op jit(solution)/shard_map/reduce_sum | solution.py:37
  18.9 0.0 copy-done.5
  18.9 0.0 copy-done.6
  18.9 0.0 copy-done.7
  18.9 0.0 copy-start.2
  18.9 2.5 %all-reduce.1 = (f32[256]{0:T(256)S(1)}, f32[256]{0:T(256)S(1)}) all-reduce(f32[256]{0:T(256)S(1)} %get-tuple-element.41, f32[256]{0:T(256)S(1)} %get-tuple-element.40), channel_id=1, replica_groups=mesh['sp'=16,'tp'=2] {'tp'}, use_global_device_ids=true, to_apply=%region_3.0 | all-reduce | flops 512 | bytes 4096 | tf_op jit(solution)/shard_map/psum | solution.py:37
  21.4 0.0 copy-done
  21.4 0.0 copy-done.8
  21.4 0.0 copy-done.9
  21.4 5.5 %multiply_reduce_fusion = (f32[1024]{0:T(1024)}, f32[256]{0:T(256)S(1)}, f32[256]{0:T(256)S(1)}, f32[1024]{0:T(1024)}, f32[256,1024]{1,0:T(8,128)}) fusion(f32[256,1024]{1,0:T(8,128)S(1)} %get-tuple-element.49, f32[256]{0:T(256)S(1)} %get-tuple-element.88, f32[256]{0:T(256)S(1)} %get-tuple-element.87, f32[1024]{0:T(1024)S(1)} %copy-done.8, ...), kind=kOutput, calls=%fused_computation.150 | convolution fusion | flops 1078720000 | bytes 7360512 | tf_op jit(solution)/shard_map/dot_general | solution.py:43
  26.9 0.0 copy-done.2
  26.9 2.4 %all-reduce = (f32[256]{0:T(256)S(1)}, f32[256]{0:T(256)S(1)}) all-reduce(f32[256]{0:T(256)S(1)} %get-tuple-element.37, f32[256]{0:T(256)S(1)} %get-tuple-element.38), channel_id=1, replica_groups=mesh['sp'=16,'tp'=2] {'tp'}, use_global_device_ids=true, to_apply=%region_7.0 | all-reduce | flops 512 | bytes 4096 | tf_op jit(solution)/shard_map/psum | solution.py:49
  29.4 4.8 %multiply_reduce_fusion.1 = (f32[1024]{0:T(1024)}, f32[1024]{0:T(1024)}, f32[1024]{0:T(1024)}, f32[1024]{0:T(1024)}, f32[1024]{0:T(1024)}, /*index=5*/f32[1024]{...) fusion(f32[286,1024]{1,0:T(8,128)S(1)} %maximum_convert_fusion,, ...), kind=kLoop, calls=%fused_computation.151 | loop fusion | flops 11515904 | bytes 22102016 | tf_op jit(solution)/shard_map/reduce_sum | solution.py:75
  34.2 2.4 %multiply_reduce_fusion.2 = (f32[1024]{0:T(1024)}, f32[1024]{0:T(1024)}, f32[1024]{0:T(1024)}, f32[1024]{0:T(1024)}, f32[1024]{0:T(1024)}, /*index=5*/f32[1024]{...) fusion(f32[256,1024]{1,0:T(8,128)S(1)} %get-tuple-element.46, ...), kind=kLoop, calls=%fused_computation.152 | loop fusion | flops 6802432 | bytes 14733312 | tf_op jit(solution)/shard_map/reduce_sum | solution.py:75
  36.6 3.9 %concatenate.44 = f32[33,1024]{1,0:T(8,128)S(1)} concatenate(f32[1,1024]{1,0:T(1,128)} %bitcast.160, f32[1,1024]{1,0:T(1,128)} %bitcast.159, f32[1,1024]{1,0:T(1,128)} %bitcast.158, f32[1,1024]{1,0:T(1,128)} %bitcast.157, f32[1,1024]{1,0:T(1,128)} %bitcast.156, f32[1,1024]{1,0:T(1,128)} %bitcast.155, f32[1,1024]{1,0:T(1,128)} %bitcast.154, f32[1,1024]{1,0:T(1,128)} %bitcast.153, ...), dimensions={0} | concatenate | bytes 270336 | tf_op jit(solution)/shard_map/concatenate | solution.py:79
  40.6 2.5 %collective-permute-start.4 = (f32[33,1024]{1,0:T(8,128)S(1)}, f32[33,1024]{1,0:T(8,128)S(1)}, u32[]{:S(2)}, u32[]{:S(2)}) collective-permute-start(f32[33,1024]{1,0:T(8,128)S(1)} %broadcast_multiply_fusion), channel_id=1, source_target_pairs={{0,2},{2,0},{4,6},{6,4},{8,10},{10,8},{12,14},{14,12},{16,18},{18,... | collective-permute-start | bytes 405512 | tf_op jit(solution)/shard_map/ppermute | solution.py:86
  43.0 4.5 %collective-permute-done.4 = f32[33,1024]{1,0:T(8,128)S(1)} collective-permute-done((f32[33,1024]{1,0:T(8,128)S(1)}, f32[33,1024]{1,0:T(8,128)S(1)}, u32[]{:S(2)}, u32[]{:S(2)}) %collective-permute-start.4) | collective-permute-done | bytes 135200 | tf_op jit(solution)/shard_map/ppermute | solution.py:86
  47.6 2.5 %collective-permute-start.5 = (f32[33,1024]{1,0:T(8,128)S(1)}, f32[33,1024]{1,0:T(8,128)S(1)}, u32[]{:S(2)}, u32[]{:S(2)}) collective-permute-start(f32[33,1024]{1,0:T(8,128)S(1)} %fusion.93), channel_id=1, source_target_pairs={{0,4},{2,6},{4,0},{6,2},{8,12},{10,14},{12,8},{14,10},{16,20},{18,... | collective-permute-start | bytes 405512 | tf_op jit(solution)/shard_map/ppermute | solution.py:86
  50.1 1.3 %collective-permute-start.2 = (f32[15,1024]{1,0:T(8,128)S(1)}, f32[15,1024]{1,0:T(8,128)S(1)}, u32[]{:S(2)}, u32[]{:S(2)}) collective-permute-start(f32[15,1024]{1,0:T(8,128)S(1)} %get-tuple-element.50), channel_id=1, source_target_pairs={{2,0},{4,2},{6,4},{8,6},{10,8},{12,10},{14,12},{16,14},{18,16},{20... | collective-permute-start | bytes 184328 | tf_op jit(solution)/shard_map/ppermute | solution.py:18
  51.4 4.5 %collective-permute-start.3 = (f32[15,1024]{1,0:T(8,128)S(1)}, f32[15,1024]{1,0:T(8,128)S(1)}, u32[]{:S(2)}, u32[]{:S(2)}) collective-permute-start(f32[15,1024]{1,0:T(8,128)S(1)} %get-tuple-element.51), channel_id=1, source_target_pairs={{0,2},{2,4},{4,6},{6,8},{8,10},{10,12},{12,14},{14,16},{16,18},{18... | collective-permute-start | bytes 184328 | tf_op jit(solution)/shard_map/ppermute | solution.py:15
  56.0 0.0 collective-permute-done.5
  56.0 1.6 %collective-permute-start.6 = (f32[33,1024]{1,0:T(8,128)S(1)}, f32[33,1024]{1,0:T(8,128)}, u32[]{:S(2)}, u32[]{:S(2)}) collective-permute-start(f32[33,1024]{1,0:T(8,128)S(1)} %add.291), channel_id=1, source_target_pairs={{0,8},{2,10},{4,12},{6,14},{8,0},{10,2},{12,4},{14,6},{16,24},{18,... | collective-permute-start | bytes 405512 | tf_op jit(solution)/shard_map/ppermute | solution.py:86
  57.6 0.0 collective-permute-done.2
  57.6 0.2 collective-permute-done.3
  57.8 0.0 copy-done.1
  57.8 6.6 %fusion.4 = (bf16[256,1024]{1,0:T(8,128)(2,1)}, f32[256,1024]{1,0:T(8,128)}) fusion(bf16[256,1024]{1,0:T(8,128)(2,1)S(1)} %copy-done.3, bf16[256,1024]{1,0:T(8,128)(2,1)S(1)} %copy-done.1, f32[256,1024]{1,0:T(8,128)S(1)} %get-tuple-element.46, f32[15,1024]{1,0:T(8,128)S(1)} %collective-permute-done.3, f32[1024]{0:T(1024)} %bitcast.127, f32[1024]{0:T(1024)} %bitcast.129, ...), kind=kLoop, calls=%fused_computation.35 | loop fusion | flops 26476544 | bytes 3919872 | tf_op jit(solution)/shard_map/convert_element_type | solution.py:91
  64.4 0.0 collective-permute-done.6
  64.4 0.9 %add.292 = f32[33,1024]{1,0:T(8,128)S(1)} add(f32[33,1024]{1,0:T(8,128)S(1)} %add.291, f32[33,1024]{1,0:T(8,128)} %collective-permute-done.6) | non-fusion elementwise | flops 33792 | bytes 405504 | tf_op jit(solution)/shard_map/add | solution.py:86
  65.4 5.9 %collective-permute-start.7 = (f32[33,1024]{1,0:T(8,128)S(1)}, f32[33,1024]{1,0:T(8,128)S(1)}, u32[]{:S(2)}, u32[]{:S(2)}) collective-permute-start(f32[33,1024]{1,0:T(8,128)S(1)} %add.292), channel_id=1, source_target_pairs={{0,16},{2,18},{4,20},{6,22},{8,24},{10,26},{12,28},{14,30},{16,0},... | collective-permute-start | bytes 405512 | tf_op jit(solution)/shard_map/ppermute | solution.py:86
  71.2 2.3 %multiply_convert_fusion = bf16[256,1024]{1,0:T(8,128)(2,1)} fusion(f32[256,1024]{1,0:T(8,128)} %get-tuple-element.48, bf16[256,1024]{1,0:T(8,128)(2,1)S(1)} %copy-done.1), kind=kLoop, calls=%fused_computation.182 | loop fusion | flops 1572864 | bytes 2097152 | tf_op jit(solution)/shard_map/convert_element_type | solution.py:90
  73.5 3.5 %collective-permute-done.7 = f32[33,1024]{1,0:T(8,128)S(1)} collective-permute-done((f32[33,1024]{1,0:T(8,128)S(1)}, f32[33,1024]{1,0:T(8,128)S(1)}, u32[]{:S(2)}, u32[]{:S(2)}) %collective-permute-start.7) | collective-permute-done | bytes 135200 | tf_op jit(solution)/shard_map/ppermute | solution.py:86
  77.0 0.6 fusion.97
  77.6 0.7 slice.579
  (12 shorter events, 0.2 us)
Async XLA Ops:
  0.6 20.8 %copy-start = (bf16[256,2048]{1,0:T(8,128)(2,1)S(1)}, bf16[256,2048]{1,0:T(8,128)(2,1)}, u32[]{:S(2)}) copy-start(bf16[256,2048]{1,0:T(8,128)(2,1)} %param.13) | copy-start | bytes 3145732
  0.6 7.8 %copy-start.4 = (f32[31,1024]{1,0:T(8,128)S(1)}, f32[31,1024]{1,0:T(8,128)}, u32[]{:S(2)}) copy-start(f32[31,1024]{1,0:T(8,128)} %param.9) | copy-start | bytes 380932
  2.3 6.5 %collective-permute-start = (bf16[15,1024]{1,0:T(8,128)(2,1)S(1)}, bf16[15,1024]{1,0:T(8,128)(2,1)S(1)}, u32[]{:S(2)}, u32[]{:S(2)}) collective-permute-start(bf16[15,1024]{1,0:T(8,128)(2,1)S(1)} %get-tuple-element.52), channel_id=1, source_target_pairs={{0,2},{2,4},{4,6},{6,8},{8,10},{10,12},{12,14},{14,16},{16,18},{18... | collective-permute-start | bytes 92168 | tf_op jit(solution)/shard_map/ppermute | solution.py:15
  7.2 5.8 %collective-permute-start.1 = (bf16[15,1024]{1,0:T(8,128)(2,1)S(1)}, bf16[15,1024]{1,0:T(8,128)(2,1)S(1)}, u32[]{:S(2)}, u32[]{:S(2)}) collective-permute-start(bf16[15,1024]{1,0:T(8,128)(2,1)S(1)} %get-tuple-element.53), channel_id=1, source_target_pairs={{2,0},{4,2},{6,4},{8,6},{10,8},{12,10},{14,12},{16,14},{18,16},{20... | collective-permute-start | bytes 92168 | tf_op jit(solution)/shard_map/ppermute | solution.py:18
  8.6 10.3 %copy-start.5 = (f32[1,1024]{1,0:T(1,128)}, f32[1,1024]{1,0:T(1,128)S(1)}, u32[]{:S(2)}) copy-start(f32[1,1024]{1,0:T(1,128)S(1)} %get-tuple-element.84) | copy-start | bytes 12292
  8.6 10.3 %copy-start.6 = (f32[1,1024]{1,0:T(1,128)}, f32[1,1024]{1,0:T(1,128)S(1)}, u32[]{:S(2)}) copy-start(f32[1,1024]{1,0:T(1,128)S(1)} %get-tuple-element.85) | copy-start | bytes 12292
  8.6 10.3 %copy-start.7 = (f32[1,1024]{1,0:T(1,128)}, f32[1,1024]{1,0:T(1,128)S(1)}, u32[]{:S(2)}) copy-start(f32[1,1024]{1,0:T(1,128)S(1)} %get-tuple-element.86) | copy-start | bytes 12292
  13.1 8.2 %copy-start.8 = (f32[1024]{0:T(1024)S(1)}, f32[1024]{0:T(1024)}, u32[]{:S(2)}) copy-start(f32[1024]{0:T(1024)} %param.10) | copy-start | bytes 12292
  13.2 8.2 %copy-start.9 = (f32[1024]{0:T(1024)S(1)}, f32[1024]{0:T(1024)}, u32[]{:S(2)}) copy-start(f32[1024]{0:T(1024)} %param.11) | copy-start | bytes 12292
  18.9 8.0 %copy-start.2 = (f32[256,1024]{1,0:T(8,128)}, f32[256,1024]{1,0:T(8,128)S(1)}, u32[]{:S(2)}) copy-start(f32[256,1024]{1,0:T(8,128)S(1)} %get-tuple-element.49) | copy-start | bytes 3145732
  36.6 21.2 %copy-start.1 = (bf16[256,1024]{1,0:T(8,128)(2,1)S(1)}, bf16[256,1024]{1,0:T(8,128)(2,1)}, u32[]{:S(2)}) copy-start(bf16[256,1024]{1,0:T(8,128)(2,1)} %param.8) | copy-start | bytes 1572868
  36.6 21.2 %copy-start.3 = (bf16[256,1024]{1,0:T(8,128)(2,1)S(1)}, bf16[256,1024]{1,0:T(8,128)(2,1)}, u32[]{:S(2)}) copy-start(bf16[256,1024]{1,0:T(8,128)(2,1)} %param.7) | copy-start | bytes 1572868
  40.6 7.0 %collective-permute-start.4 = (f32[33,1024]{1,0:T(8,128)S(1)}, f32[33,1024]{1,0:T(8,128)S(1)}, u32[]{:S(2)}, u32[]{:S(2)}) collective-permute-start(f32[33,1024]{1,0:T(8,128)S(1)} %broadcast_multiply_fusion), channel_id=1, source_target_pairs={{0,2},{2,0},{4,6},{6,4},{8,10},{10,8},{12,14},{14,12},{16,18},{18,... | collective-permute-start | bytes 405512 | tf_op jit(solution)/shard_map/ppermute | solution.py:86
  47.6 8.4 %collective-permute-start.5 = (f32[33,1024]{1,0:T(8,128)S(1)}, f32[33,1024]{1,0:T(8,128)S(1)}, u32[]{:S(2)}, u32[]{:S(2)}) collective-permute-start(f32[33,1024]{1,0:T(8,128)S(1)} %fusion.93), channel_id=1, source_target_pairs={{0,4},{2,6},{4,0},{6,2},{8,12},{10,14},{12,8},{14,10},{16,20},{18,... | collective-permute-start | bytes 405512 | tf_op jit(solution)/shard_map/ppermute | solution.py:86
  50.1 7.5 %collective-permute-start.2 = (f32[15,1024]{1,0:T(8,128)S(1)}, f32[15,1024]{1,0:T(8,128)S(1)}, u32[]{:S(2)}, u32[]{:S(2)}) collective-permute-start(f32[15,1024]{1,0:T(8,128)S(1)} %get-tuple-element.50), channel_id=1, source_target_pairs={{2,0},{4,2},{6,4},{8,6},{10,8},{12,10},{14,12},{16,14},{18,16},{20... | collective-permute-start | bytes 184328 | tf_op jit(solution)/shard_map/ppermute | solution.py:18
  51.4 6.4 %collective-permute-start.3 = (f32[15,1024]{1,0:T(8,128)S(1)}, f32[15,1024]{1,0:T(8,128)S(1)}, u32[]{:S(2)}, u32[]{:S(2)}) collective-permute-start(f32[15,1024]{1,0:T(8,128)S(1)} %get-tuple-element.51), channel_id=1, source_target_pairs={{0,2},{2,4},{4,6},{6,8},{8,10},{10,12},{12,14},{14,16},{16,18},{18... | collective-permute-start | bytes 184328 | tf_op jit(solution)/shard_map/ppermute | solution.py:15
  56.0 8.4 %collective-permute-start.6 = (f32[33,1024]{1,0:T(8,128)S(1)}, f32[33,1024]{1,0:T(8,128)}, u32[]{:S(2)}, u32[]{:S(2)}) collective-permute-start(f32[33,1024]{1,0:T(8,128)S(1)} %add.291), channel_id=1, source_target_pairs={{0,8},{2,10},{4,12},{6,14},{8,0},{10,2},{12,4},{14,6},{16,24},{18,... | collective-permute-start | bytes 405512 | tf_op jit(solution)/shard_map/ppermute | solution.py:86
  65.4 11.6 %collective-permute-start.7 = (f32[33,1024]{1,0:T(8,128)S(1)}, f32[33,1024]{1,0:T(8,128)S(1)}, u32[]{:S(2)}, u32[]{:S(2)}) collective-permute-start(f32[33,1024]{1,0:T(8,128)S(1)} %add.292), channel_id=1, source_target_pairs={{0,16},{2,18},{4,20},{6,22},{8,24},{10,26},{12,28},{14,30},{16,0},... | collective-permute-start | bytes 405512 | tf_op jit(solution)/shard_map/ppermute | solution.py:86
